TPU v7x, 32 devices: a whole 2x2x4 slice. The times are simulated.
32 devices in a mesh: rep: 2 (over x), fs: 8 (over z, y), tp: 2 (over core).
Axes of the slice: x: 2, y: 2, z: 4, core: 2. Of those that a mesh axis runs over, the one named last changes fastest.
Arguments:
- inputs_next: bfloat16 [2048, 2048], P(('rep', 'fs'), 'tp'), parts along dimension 0, may hold values from -6 to 6
- inputs_prev: bfloat16 [2048, 2048], P(('rep', 'fs'), 'tp'), parts along dimension 0, may hold values from -6 to 6
- hidden_prev: bfloat16 [2048, 8192], P(('rep', 'fs')), parts along dimension 0, may hold values from -6 to 6
- cotangent: bfloat16 [2048, 2048], P(('rep', 'fs'), 'tp'), parts along dimension 0, may hold values from -6 to 6
- up_weight: bfloat16 [2048, 8192], P('tp', 'fs'), may hold values from -0.125 to 0.125
- down_weight: bfloat16 [8192, 2048], P('fs', 'tp'), may hold values from -0.0625 to 0.0625
- up_accum: float32 [4096, 8192], P(('rep', 'tp'), 'fs'), parts along dimension 0, may hold values from -192 to 192
- down_accum: float32 [16384, 2048], P(('rep', 'fs'), 'tp'), parts along dimension 0, may hold values from -192 to 192
Outputs:
- output_next: bfloat16 [2048, 2048], P(('rep', 'fs'), 'tp'), parts along dimension 0
- hidden_next: bfloat16 [2048, 8192], P(('rep', 'fs')), parts along dimension 0
- input_grad: bfloat16 [2048, 2048], P(('rep', 'fs'), 'tp'), parts along dimension 0
- up_accum_out: float32 [4096, 8192], P(('rep', 'tp'), 'fs'), parts along dimension 0
- down_accum_out: float32 [16384, 2048], P(('rep', 'fs'), 'tp'), parts along dimension 0
There are 2 independent parts, one for each index of `rep`. A program takes and returns all parts, laid end to end along the dimension named above; an argument that names none is the same for every part. Nothing has to cross between parts.
All inputs are finite; a program needn't handle non-finite values.
Results may differ from a plain program's by a relative error of at most 0.034.
Values may be sent and summed in bfloat16 or wider, within the bound.
A program may use at most 128 MiB of HBM per device.

v0:
```python
import jax
import jax.numpy as jnp
from jax import lax
from jax.sharding import PartitionSpec as P


def squared_relu(values):
    return jnp.square(jax.nn.relu(values.astype(jnp.float32))).astype(jnp.bfloat16)


def contract(left, right, left_dim, right_dim):
    return lax.dot_general(
        left, right, (((left_dim,), (right_dim,)), ((), ())), preferred_element_type=jnp.float32
    )


def local(
    inputs_next, inputs_prev, hidden_prev, cotangent, up_weight, down_weight, up_accum, down_accum
):
    up_whole = lax.all_gather(up_weight, "fs", axis=1, tiled=True)
    hidden_terms = jnp.dot(inputs_next, up_whole, preferred_element_type=jnp.float32).astype(
        jnp.bfloat16
    )
    hidden_next = lax.psum(hidden_terms, "tp").astype(jnp.float32).astype(jnp.bfloat16)
    acts_next = squared_relu(hidden_next)
    saved_inputs, cotangent_all = (
        lax.all_gather(inputs_prev, "fs", axis=0, tiled=True),
        lax.all_gather(cotangent, "fs", axis=0, tiled=True),
    )
    acts_rows = lax.all_to_all(acts_next, "fs", split_axis=1, concat_axis=0, tiled=True)
    output_next = lax.psum_scatter(
        jnp.dot(acts_rows, down_weight, preferred_element_type=jnp.float32).astype(jnp.bfloat16),
        "fs",
        scatter_dimension=0,
        tiled=True,
    )
    saved_spread = lax.all_to_all(hidden_prev, "fs", split_axis=1, concat_axis=0, tiled=True)
    acts_spread = squared_relu(saved_spread)
    back_terms = contract(cotangent_all, down_weight, 1, 1).astype(jnp.bfloat16)
    back_sum = lax.psum(back_terms, "tp").astype(jnp.float32)
    grad_spread = (back_sum * 2.0 * jax.nn.relu(saved_spread.astype(jnp.float32))).astype(
        jnp.bfloat16
    )
    hidden_grad = lax.all_to_all(grad_spread, "fs", split_axis=0, concat_axis=1, tiled=True)
    input_grad = contract(hidden_grad, up_whole, 1, 1).astype(jnp.bfloat16)
    up_accum_out = up_accum + contract(saved_inputs, grad_spread, 0, 0)
    down_accum_out = down_accum + contract(acts_spread, cotangent_all, 0, 0)
    return (output_next, hidden_next, input_grad, up_accum_out, down_accum_out)


def solution(mesh):
    return jax.shard_map(
        local,
        mesh=mesh,
        in_specs=(
            P(("rep", "fs"), "tp"),
            P(("rep", "fs"), "tp"),
            P(("rep", "fs"), None),
            P(("rep", "fs"), "tp"),
            P("tp", "fs"),
            P("fs", "tp"),
            P(("rep", "tp"), "fs"),
            P(("rep", "fs"), "tp"),
        ),
        out_specs=(
            P(("rep", "fs"), "tp"),
            P(("rep", "fs"), None),
            P(("rep", "fs"), "tp"),
            P(("rep", "tp"), "fs"),
            P(("rep", "fs"), "tp"),
        ),
        check_vma=False,
    )
```

profile of v0, /device:TPU:0, one launch (start us, length us, event | category | flops | bytes accessed | tf_op | source)
XLA Modules:
  0.0 542.0 jit_solution(11550131855770351500)
XLA Ops:
  8.7 53.2 %all-gather.6.cloned.1.call-done = bf16[1024,1024]{1,0:T(8,128)(2,1)} async-done(((bf16[128,1024]{1,0:T(8,128)(2,1)}), bf16[1024,1024]{1,0:T(8,128)(2,1)}) %all-gather.6.cloned.1.call-update) | async-done | bytes 2097168 | tf_op jit(solution)/shard_map/all_gather | solution.py:28
  62.0 5.3 convolution_convert_fusion.1
  67.2 222.7 %all-gather.4.cloned.1.call-done = bf16[1024,8192]{1,0:T(8,128)(2,1)} async-done(((bf16[1024,1024]{1,0:T(8,128)(2,1)}), bf16[1024,8192]{1,0:T(8,128)(2,1)}) %all-gather.4.cloned.1.call-update) | async-done | bytes 16777232 | tf_op jit(solution)/shard_map/all_gather | solution.py:20
  290.0 9.4 %convolution_convert_fusion = bf16[128,8192]{1,0:T(8,128)(2,1)} fusion(bf16[128,1024]{1,0:T(8,128)(2,1)S(1)} %copy-done.5, bf16[1024,8192]{1,0:T(8,128)(2,1)} %all-gather.4.cloned.1.call-done), kind=kOutput, calls=%fused_computation | convolution fusion | flops 2148532224 | bytes 19136512 | tf_op jit(solution)/shard_map/dot_general | solution.py:21
  299.4 3.2 copy.25
  302.6 4.3 all-to-all-start.1
  306.9 19.2 %all-reduce.3.cloned.1.call-done = (bf16[128,8192]{1,0:T(8,128)(2,1)}, bf16[1024,1024]{1,0:T(8,128)(2,1)}) async-done(((bf16[128,8192]{1,0:T(8,128)(2,1)}, bf16[1024,1024]{1,0:T(8,128)(2,1)}), (bf16[128,8192]{1,0:T(8,128)(2,1)}, bf16[1024,1024]{1,0:T(8,128)(2,1)})) %all-reduce.3.cloned.1.call-update) | async-done | bytes 4194320 | tf_op jit(solution)/shard_map/psum | solution.py:24
  326.1 2.1 multiply_convert_fusion
  329.7 25.1 %all-to-all-done.1 = bf16[128,8,1024]{2,0,1:T(8,128)(2,1)} async-done(((bf16[128,8,1024]{2,0,1:T(8,128)(2,1)}), bf16[128,8,1024]{2,0,1:T(8,128)(2,1)}, u32[]{:S(2)}, u32[]{:S(2)}) %all-to-all-start.1) | async-done | bytes 2097184 | tf_op jit(solution)/shard_map/all_to_all | solution.py:37
  354.8 4.4 all-to-all-start
  359.8 2.3 convert_maximum_fusion
  362.1 3.2 fusion.1
  365.3 3.9 copy.18
  369.2 59.6 %all-to-all-done = bf16[128,8,1024]{2,0,1:T(8,128)(2,1)} async-done(((bf16[128,8,1024]{2,0,1:T(8,128)(2,1)}), bf16[128,8,1024]{2,0,1:T(8,128)(2,1)}, u32[]{:S(2)}, u32[]{:S(2)}) %all-to-all-start) | async-done | bytes 2097184 | tf_op jit(solution)/shard_map/all_to_all | solution.py:30
  428.8 4.3 all-to-all-start.2
  433.4 5.2 convolution_convert_fusion.2
  438.6 5.5 %copy.19 = f32[1024,1024]{0,1:T(8,128)} copy(f32[1024,1024]{1,0:T(8,128)} %param.14) | data formatting | bytes 8388608 | tf_op args[6]
  444.1 7.2 %bitcast_add_fusion = f32[1024,1024]{0,1:T(8,128)} fusion(f32[1024,1024]{0,1:T(8,128)} %copy.19, bf16[1024,1024]{1,0:T(8,128)(2,1)S(1)} %copy-done.2, bf16[1024,1024]{1,0:T(8,128)(2,1)} %all-gather.8.cloned.1.call-done), kind=kOutput, calls=%fused_computation.5 | convolution fusion | flops 2148532224 | bytes 12582912 | tf_op jit(solution)/shard_map/dot_general | solution.py:12
  451.4 5.5 %copy.20 = f32[1024,1024]{1,0:T(8,128)} copy(f32[1024,1024]{0,1:T(8,128)} %bitcast_add_fusion) | data formatting | bytes 8388608
  456.9 7.3 %convolution_add_fusion = f32[1024,1024]{1,0:T(8,128)} fusion(f32[1024,1024]{1,0:T(8,128)} %param.15, bf16[1024,1024]{1,0:T(8,128)(2,1)S(1)} %copy-done.4, bf16[1024,1024]{1,0:T(8,128)(2,1)} %all-gather.6.cloned.1.call-done), kind=kOutput, calls=%fused_computation.10 | convolution fusion | flops 2148532224 | bytes 12582912 | tf_op jit(solution)/shard_map/dot_general | solution.py:12
  464.1 32.6 %all-to-all-done.2 = bf16[8,128,1024]{1,2,0:T(8,128)(2,1)} async-done(((bf16[8,128,1024]{1,2,0:T(8,128)(2,1)}), bf16[8,128,1024]{1,2,0:T(8,128)(2,1)}, u32[]{:S(2)}, u32[]{:S(2)}) %all-to-all-start.2) | async-done | bytes 2097184 | tf_op jit(solution)/shard_map/all_to_all | solution.py:44
  496.7 13.1 %convolution_convert_fusion.3 = bf16[128,1024]{1,0:T(8,128)(2,1)} fusion(bf16[128,8192]{0,1:T(8,128)(2,1)} %bitcast.6, bf16[1024,8192]{1,0:T(8,128)(2,1)} %all-gather.4.cloned.1.call-done), kind=kOutput, calls=%fused_computation.13 | convolution fusion | flops 2147614720 | bytes 19136512 | tf_op jit(solution)/shard_map/dot_general | solution.py:12
  509.8 22.5 %reduce-scatter.2.cloned.1.call-done = bf16[128,1024]{1,0:T(8,128)(2,1)} async-done(((bf16[1024,1024]{1,0:T(8,128)(2,1)}), bf16[128,1024]{1,0:T(8,128)(2,1)}) %reduce-scatter.2.cloned.1.call-update) | async-done | bytes 262160 | tf_op jit(solution)/shard_map/reduce_scatter | solution.py:31
  532.3 3.1 copy.29
  (24 shorter events, 3.8 us)
Async XLA Ops:
  7.2 54.8 %copy-start = (bf16[1024,1024]{1,0:T(8,128)(2,1)S(1)}, bf16[1024,1024]{1,0:T(8,128)(2,1)}, u32[]{:S(2)}) copy-start(bf16[1024,1024]{1,0:T(8,128)(2,1)} %param.13) | copy-start | bytes 6291460
  7.2 54.8 %all-gather.6.cloned.1.call-start = ((), (), s32[]{:S(2)}) async-start(), calls=%async_computation.6 | async-start | bytes 2359296 | tf_op jit(solution)/shard_map/all_gather | solution.py:28
  7.9 282.1 %all-gather.4.cloned.1.call-start = ((), (), s32[]{:S(2)}) async-start(), calls=%async_computation.4 | async-start | bytes 18874368 | tf_op jit(solution)/shard_map/all_gather | solution.py:20
  8.7 281.3 %copy-start.5 = (bf16[128,1024]{1,0:T(8,128)(2,1)S(1)}, bf16[128,1024]{1,0:T(8,128)(2,1)}, u32[]{:S(2)}) copy-start(bf16[128,1024]{1,0:T(8,128)(2,1)} %param.8) | copy-start | bytes 786436
  8.7 317.5 %all-reduce.3.cloned.1.call-start = ((), (), s32[]{:S(2)}) async-start(), calls=%async_computation.8 | async-start | bytes 8388608 | tf_op jit(solution)/shard_map/psum | solution.py:24
  302.6 52.2 %all-to-all-start.1 = ((bf16[128,8,1024]{2,0,1:T(8,128)(2,1)}), bf16[128,8,1024]{2,0,1:T(8,128)(2,1)}, u32[]{:S(2)}, u32[]{:S(2)}) async-start(bf16[128,8,1024]{2,0,1:T(8,128)(2,1)} %bitcast.40), calls=%async_computation.2 | async-start | bytes 4194304 | tf_op jit(solution)/shard_map/all_to_all | solution.py:37
  354.8 74.0 %all-to-all-start = ((bf16[128,8,1024]{2,0,1:T(8,128)(2,1)}), bf16[128,8,1024]{2,0,1:T(8,128)(2,1)}, u32[]{:S(2)}, u32[]{:S(2)}) async-start(bf16[128,8,1024]{2,0,1:T(8,128)(2,1)} %bitcast.39), calls=%async_computation | async-start | bytes 4194304 | tf_op jit(solution)/shard_map/all_to_all | solution.py:30
  359.2 84.9 %all-gather.8.cloned.1.call-start = ((), (), s32[]{:S(2)}) async-start(), calls=%async_computation.7 | async-start | bytes 2359296 | tf_op jit(solution)/shard_map/all_gather | solution.py:27
  359.8 2.3 copy-start.3
  428.8 67.9 %all-to-all-start.2 = ((bf16[8,128,1024]{1,2,0:T(8,128)(2,1)}), bf16[8,128,1024]{1,2,0:T(8,128)(2,1)}, u32[]{:S(2)}, u32[]{:S(2)}) async-start(bf16[8,128,1024]{1,2,0:T(8,128)(2,1)} %copy.18), calls=%async_computation.3 | async-start | bytes 4194304 | tf_op jit(solution)/shard_map/all_to_all | solution.py:44
  433.1 99.2 %reduce-scatter.2.cloned.1.call-start = ((), (), s32[]{:S(2)}) async-start(), calls=%async_computation.5 | async-start | bytes 2359296 | tf_op jit(solution)/shard_map/reduce_scatter | solution.py:31
  438.6 5.5 %copy-start.2 = (bf16[1024,1024]{1,0:T(8,128)(2,1)S(1)}, bf16[1024,1024]{1,0:T(8,128)(2,1)}, u32[]{:S(2)}) copy-start(bf16[1024,1024]{1,0:T(8,128)(2,1)} %get-tuple-element.18) | copy-start | bytes 6291460
  451.4 5.5 %copy-start.4 = (bf16[1024,1024]{1,0:T(8,128)(2,1)S(1)}, bf16[1024,1024]{1,0:T(8,128)(2,1)}, u32[]{:S(2)}) copy-start(bf16[1024,1024]{1,0:T(8,128)(2,1)} %get-tuple-element.17) | copy-start | bytes 6291460
  496.7 38.7 %copy-start.1 = (bf16[1024,1024]{1,0:T(8,128)(2,1)S(1)}, bf16[1024,1024]{1,0:T(8,128)(2,1)}, u32[]{:S(2)}) copy-start(bf16[1024,1024]{1,0:T(8,128)(2,1)} %param.13) | copy-start | bytes 6291460
Sparse Core Ops, SparseCore 0:
  10.1 51.7 all-gather.5
  64.1 225.7 all-gather.3
  299.6 26.5 all-reduce.2
  361.8 70.7 all-gather.7
  438.7 93.5 reduce-scatter.1
where the time goes:
time: 543 us; the launch traced here: 542 us
  waiting for transfers between devices  437 us (80%)
  matrix products  47.6 us (9%)
  local copies, waits for them, and re-layouts  22.7 us (4%)
  between operations  13.9 us (3%)
  starting transfers between devices  13.4 us (2%)
  other arithmetic  7.57 us (1%)
    all_gather x1, waiting for transfers between devices, local(): up_whole = lax.all_gather(up_weight, 'fs', axis=1, tiled=True)  223 us
    all_to_all x1, waiting for transfers between devices, local(): lax.all_to_all(acts_next, 'fs', split_axis=1, concat_axis=0, tiled=True)  59.6 us
    all_gather x1, waiting for transfers between devices, local(): lax.all_gather(cotangent, 'fs', axis=0, tiled=True)  53.2 us
    dot_general x4, matrix products, contract(): lax.dot_general(left, right, (((left_dim,), (right_dim,)), ((), ())), pre...  32.9 us
    all_to_all x1, waiting for transfers between devices, local(): lax.all_to_all(grad_spread, 'fs', split_axis=0, concat_axis=1, tiled=True)  32.6 us
    all_to_all x1, waiting for transfers between devices, local(): lax.all_to_all(hidden_prev, 'fs', split_axis=1, concat_axis=0, tiled=True)  25.1 us
    reduce_scatter x1, waiting for transfers between devices, local(): lax.psum_scatter(jnp.dot(acts_rows, down_weight, preferred_element_type=j...  22.5 us
    psum x1, waiting for transfers between devices, local(): lax.psum(hidden_terms, 'tp').astype(jnp.float32).astype(jnp.bfloat16)  19.2 us
  transfers between devices with their start and end apart: 8, of which 7 were waited for; matrix products, arithmetic and copies ran while one was open for 12% of the time, Pallas kernels for 0%

commit v1 on v0

v1 whole, which is shorter than its diff:
```python
import functools

import jax
import jax.numpy as jnp
from jax import lax
from jax.experimental import pallas as pl
from jax.experimental.pallas import tpu as pltpu
from jax.sharding import PartitionSpec as P

F32, BF16 = jnp.float32, jnp.bfloat16
PAIR = 2


def relu_squared(values):
    return jnp.square(jnp.maximum(values.astype(F32), 0.0)).astype(BF16)


def contract(left, right, left_dim, right_dim):
    return lax.dot_general(
        left, right, (((left_dim,), (right_dim,)), ((), ())), preferred_element_type=F32
    )


def send(src, dst, send_sem, recv_sem, **target):
    return pltpu.make_async_remote_copy(
        src_ref=src, dst_ref=dst, send_sem=send_sem, recv_sem=recv_sem,
        device_id=target, device_id_type=pl.DeviceIdType.MESH,
    )


def kernel(
    n_fs, n_tp, n_up, n_down,
    xn, xp, hp, ct, uw, dw, ua_hbm, da_hbm,
    out, hn, ig, uo_hbm, do_hbm,
    x_all, c_all, p_all, hp_all, h_all, hg_all,
    ht, bt, tp_h, tp_b, ot, it, ry_o, ry_i, ps_o, ps_i, rz_o, rz_i, ua, da,
    x_s, x_r, c_s, c_r, p_s, p_r, hps_s, hps_r, hpt_s, hpt_r,
    th_s, th_r, tb_s, tb_r, ah_s, ah_r, ab_s, ab_r, hna_s, hna_r, hnt_s, hnt_r,
    yo_s, yo_r, zo_s, zo_r, yi_s, yi_r, zi_s, zi_r, load_s, up_s, down_s,
):
    f, t = lax.axis_index("fs"), lax.axis_index("tp")
    n_z = n_fs // PAIR
    z, y = f // PAIR, lax.rem(f, PAIR)
    mate = z * PAIR + (1 - y)
    rows, width = xn.shape[0], dw.shape[0]
    part = rows // n_tp
    mine = pl.ds(pl.multiple_of(t * part, part), part)

    def z_peer(k):
        return lax.rem(z + k, n_z)

    def fs_peer(k):
        return lax.rem(f + k, n_fs)

    def tp_peer(k):
        return lax.rem(t + k, n_tp)

    def part_of(p):
        return pl.ds(pl.multiple_of(p * part, part), part)

    def unit(g):
        return pl.ds(pl.multiple_of(g * width, width), width)

    sent = []

    def go(copy):
        copy.start()
        sent.append(copy)

    def landed(dst, send_sem, recv_sem, **target):
        send(dst, dst, send_sem, recv_sem, **target).wait_recv()

    def gather_start(own, whole, ss, rs):
        for k in range(1, n_z):
            go(send(own, whole.at[f], ss.at[k], rs.at[f], fs=z_peer(k) * PAIR + y))
        go(send(own, whole.at[f], ss.at[0], rs.at[f], fs=mate))

    def gather_forward(own, whole, ss, rs):
        whole[f] = own[...]
        for k in range(1, n_z):
            src = z_peer(k) * PAIR + y
            landed(whole.at[src], ss.at[0], rs.at[src], fs=mate)
            go(send(whole.at[src], whole.at[src], ss.at[n_z + k - 1], rs.at[src], fs=mate))

    def gather_finish(whole, ss, rs):
        for k in range(n_z):
            src = z_peer(k) * PAIR + (1 - y)
            landed(whole.at[src], ss.at[0], rs.at[src], fs=mate)

    def tp_scatter(terms, held, ss, rs):
        for k in range(1, n_tp):
            p = tp_peer(k)
            go(send(terms.at[:, part_of(p), :], held.at[t], ss.at[k], rs.at[t], tp=p))

    def tp_scatter_wait(held, ss, rs):
        for k in range(1, n_tp):
            p = tp_peer(k)
            landed(held.at[p], ss.at[0], rs.at[p], tp=p)

    def tp_gather(view, ss, rs):
        for k in range(1, n_tp):
            go(send(view(mine), view(mine), ss.at[k], rs.at[t], tp=tp_peer(k)))

    def tp_gather_wait(view, ss, rs):
        for k in range(1, n_tp):
            p = tp_peer(k)
            landed(view(part_of(p)), ss.at[0], rs.at[p], tp=p)

    def tp_total(terms, held, i):
        total = terms[i, mine, :].astype(F32)
        for k in range(1, n_tp):
            total = total + held[tp_peer(k), i].astype(F32)
        return total

    def products(left_of, right, right_dim, terms):
        @pl.loop(0, n_fs // PAIR)
        def _(i):
            left = left_of(pl.ds(i * PAIR, PAIR))
            left = left.reshape(PAIR * rows, left.shape[-1])
            total = contract(left, right[...], 1, right_dim).astype(BF16)
            terms[pl.ds(i * PAIR, PAIR)] = total.reshape(PAIR, rows, total.shape[-1])

    def scatter_start(terms, ry, ss, rs):
        for k in range(n_z):
            zz = z_peer((k + 1) % n_z)
            go(send(terms.at[zz * PAIR + (1 - y)], ry.at[zz], ss.at[k], rs.at[zz], fs=mate))

    def scatter_pass(terms, ry, ps, rz, ss, rs, zs, zr):
        for k in range(1, n_z):
            zz = z_peer(k)
            landed(ry.at[zz], ss.at[0], rs.at[zz], fs=mate)
            ps[zz] = (terms[zz * PAIR + y].astype(F32) + ry[zz].astype(F32)).astype(BF16)
            go(send(ps.at[zz], rz.at[z], zs.at[k], zr.at[z], fs=zz * PAIR + y))

    def scatter_finish(terms, ry, rz, ss, rs, zs, zr, result):
        landed(ry.at[z], ss.at[0], rs.at[z], fs=mate)
        total = terms[f].astype(F32) + ry[z].astype(F32)
        for k in range(1, n_z):
            zz = z_peer(k)
            landed(rz.at[zz], zs.at[0], zr.at[zz], fs=zz * PAIR + y)
            total = total + rz[zz].astype(F32)
        result[...] = total.astype(BF16)

    barrier = pltpu.get_barrier_semaphore()
    for k in range(1, n_fs):
        pl.semaphore_signal(
            barrier, inc=1, device_id={"fs": fs_peer(k)}, device_id_type=pl.DeviceIdType.MESH
        )
    for k in range(1, n_tp):
        pl.semaphore_signal(
            barrier, inc=1, device_id={"tp": tp_peer(k)}, device_id_type=pl.DeviceIdType.MESH
        )
    pl.semaphore_wait(barrier, n_fs + n_tp - 2)

    gather_start(xn, x_all, x_s, x_r)
    gather_start(ct, c_all, c_s, c_r)
    for k in range(1, n_fs):
        g = fs_peer(k)
        go(send(hp.at[mine, unit(g)], hp_all.at[f, mine, :], hps_s.at[k], hps_r.at[f], fs=g))
    loads = [
        pltpu.make_async_copy(ua_hbm, ua, load_s.at[0]),
        pltpu.make_async_copy(da_hbm, da, load_s.at[1]),
    ]
    for load in loads:
        load.start()
    hp_all[f, mine, :] = hp[mine, unit(f)]

    gather_forward(xn, x_all, x_s, x_r)
    gather_finish(x_all, x_s, x_r)
    products(lambda at: x_all[at], uw, 0, ht)
    tp_scatter(ht, tp_h, th_s, th_r)
    tp_scatter_wait(tp_h, th_s, th_r)

    @pl.loop(0, n_fs)
    def _(i):
        h_all[i, mine, :] = tp_total(ht, tp_h, i).astype(BF16)

    tp_gather(lambda at: h_all.at[:, at, :], ah_s, ah_r)
    for k in range(1, n_fs):
        g = fs_peer(k)
        go(send(h_all.at[g, mine, :], hn.at[mine, unit(f)], hna_s.at[k], hna_r.at[f], fs=g))
    hn[mine, unit(f)] = h_all[f, mine, :]
    tp_gather_wait(lambda at: h_all.at[:, at, :], ah_s, ah_r)
    products(lambda at: relu_squared(h_all[at]), dw, 0, ot)
    scatter_start(ot, ry_o, yo_s, yo_r)

    gather_forward(ct, c_all, c_s, c_r)
    gather_start(xp, p_all, p_s, p_r)
    scatter_pass(ot, ry_o, ps_o, rz_o, yo_s, yo_r, zo_s, zo_r)
    gather_finish(c_all, c_s, c_r)
    products(lambda at: c_all[at], dw, 1, bt)
    tp_scatter(bt, tp_b, tb_s, tb_r)
    for k in range(1, n_fs):
        g = fs_peer(k)
        landed(hp_all.at[g, mine, :], hps_s.at[0], hps_r.at[g], fs=g)
    tp_gather(lambda at: hp_all.at[:, at, :], hpt_s, hpt_r)
    tp_scatter_wait(tp_b, tb_s, tb_r)

    @pl.loop(0, n_fs)
    def _(i):
        slope = jnp.maximum(hp_all[i, mine, :].astype(F32), 0.0)
        hg_all[i, mine, :] = (tp_total(bt, tp_b, i) * 2.0 * slope).astype(BF16)

    tp_gather(lambda at: hg_all.at[:, at, :], ab_s, ab_r)
    tp_gather_wait(lambda at: hg_all.at[:, at, :], ab_s, ab_r)
    products(lambda at: hg_all[at], uw, 1, it)
    scatter_start(it, ry_i, yi_s, yi_r)
    gather_forward(xp, p_all, p_s, p_r)

    tp_gather_wait(lambda at: hp_all.at[:, at, :], hpt_s, hpt_r)
    for load in loads:
        load.wait()

    def accumulate(left_of, right, total, hbm, sems, pieces):
        high = total.shape[0] // pieces

        def piece(i):
            return pl.ds(pl.multiple_of(i * high, high), high)

        @pl.loop(0, pieces)
        def _(i):
            left = left_of(piece(i)).reshape(n_fs * rows, high)
            flat = right[...].reshape(n_fs * rows, right.shape[-1])
            total[piece(i), :] += contract(left, flat, 0, 0)
            pltpu.make_async_copy(total.at[piece(i), :], hbm.at[piece(i), :], sems.at[i]).start()

        def drain():
            for i in range(pieces):
                at = pl.ds(i * high, high)
                pltpu.make_async_copy(total.at[at, :], hbm.at[at, :], sems.at[i]).wait()

        return drain

    drain_down = accumulate(
        lambda at: relu_squared(hp_all[:, :, at]), c_all, da, do_hbm, down_s, n_down
    )
    scatter_pass(it, ry_i, ps_i, rz_i, yi_s, yi_r, zi_s, zi_r)

    for k in range(1, n_fs):
        g = fs_peer(k)
        landed(hn.at[mine, unit(g)], hna_s.at[0], hna_r.at[g], fs=g)
    tp_gather(lambda at: hn.at[at, :], hnt_s, hnt_r)
    scatter_finish(ot, ry_o, rz_o, yo_s, yo_r, zo_s, zo_r, out)
    gather_finish(p_all, p_s, p_r)
    drain_up = accumulate(lambda at: p_all[:, :, at], hg_all, ua, uo_hbm, up_s, n_up)
    scatter_finish(it, ry_i, rz_i, yi_s, yi_r, zi_s, zi_r, ig)
    tp_gather_wait(lambda at: hn.at[at, :], hnt_s, hnt_r)
    drain_down()
    drain_up()
    for copy in sent:
        copy.wait_send()


def local(n_fs, n_tp, xn, xp, hp, ct, uw, dw, ua, da):
    rows, depth = xn.shape
    width = dw.shape[0]
    n_z = n_fs // PAIR
    part = rows // n_tp
    n_up, n_down = max(1, depth // 256), max(1, width // 256)
    dma = pltpu.SemaphoreType.DMA

    def held(*shape, dtype=BF16):
        return pltpu.VMEM(shape, dtype)

    def tokens(columns):
        return held(n_fs, rows, columns)

    vmem, anywhere = pl.BlockSpec(memory_space=pltpu.VMEM), pl.BlockSpec(memory_space=pl.ANY)
    fs_sem, tp_sem, z_sem = dma((n_fs,)), dma((n_tp,)), dma((n_z,))
    return pl.pallas_call(
        functools.partial(kernel, n_fs, n_tp, n_up, n_down),
        out_shape=(
            jax.ShapeDtypeStruct(xn.shape, BF16),
            jax.ShapeDtypeStruct(hp.shape, BF16),
            jax.ShapeDtypeStruct(xp.shape, BF16),
            jax.ShapeDtypeStruct(ua.shape, F32),
            jax.ShapeDtypeStruct(da.shape, F32),
        ),
        in_specs=[vmem] * 6 + [anywhere] * 2,
        out_specs=(vmem, vmem, vmem, anywhere, anywhere),
        scratch_shapes=[
            tokens(depth), tokens(depth), tokens(depth),
            tokens(width), tokens(width), tokens(width),
            tokens(width), tokens(width),
            held(n_tp, n_fs, part, width), held(n_tp, n_fs, part, width),
            tokens(depth), tokens(depth),
            held(n_z, rows, depth), held(n_z, rows, depth),
            held(n_z, rows, depth), held(n_z, rows, depth),
            held(n_z, rows, depth), held(n_z, rows, depth),
            held(*ua.shape, dtype=F32), held(*da.shape, dtype=F32),
            fs_sem, fs_sem, fs_sem, fs_sem, fs_sem, fs_sem, fs_sem, fs_sem, tp_sem, tp_sem,
            tp_sem, tp_sem, tp_sem, tp_sem, tp_sem, tp_sem, tp_sem, tp_sem,
            fs_sem, fs_sem, tp_sem, tp_sem,
            z_sem, z_sem, z_sem, z_sem, z_sem, z_sem, z_sem, z_sem,
            dma((2,)), dma((n_up,)), dma((n_down,)),
        ],
        compiler_params=pltpu.CompilerParams(
            collective_id=0, has_side_effects=True, vmem_limit_bytes=62 * 1024 * 1024
        ),
    )(xn, xp, hp, ct, uw, dw, ua, da)


def solution(mesh):
    return jax.shard_map(
        functools.partial(local, mesh.shape["fs"], mesh.shape["tp"]),
        mesh=mesh,
        in_specs=(
            P(("rep", "fs"), "tp"),
            P(("rep", "fs"), "tp"),
            P(("rep", "fs"), None),
            P(("rep", "fs"), "tp"),
            P("tp", "fs"),
            P("fs", "tp"),
            P(("rep", "tp"), "fs"),
            P(("rep", "fs"), "tp"),
        ),
        out_specs=(
            P(("rep", "fs"), "tp"),
            P(("rep", "fs"), None),
            P(("rep", "fs"), "tp"),
            P(("rep", "tp"), "fs"),
            P(("rep", "fs"), "tp"),
        ),
        check_vma=False,
    )
```

time: 543 us -> 202 us (0.37)
  the two profiles are of different devices: /device:TPU:0 before, /device:TPU:14 now
where the time goes in v1:
time: 202 us; the launch traced here: 201 us
  Pallas kernels  189 us (94%)
  local copies, waits for them, and re-layouts  11.3 us (6%)
    pallas_call x1, Pallas kernels, local(): pl.pallas_call(functools.partial(kernel, n_fs, n_tp, n_up, n_down), out_s...  189 us
    unnamed x11, local copies, waits for them, and re-layouts  11.3 us

profile of v1, /device:TPU:14, one launch (start us, length us, event | category | flops | bytes accessed | tf_op | source)
XLA Modules:
  0.0 201.5 jit_solution(12108269996230422143)
XLA Ops:
  0.6 189.5 %shard_map.119 = (bf16[128,1024]{1,0:T(8,128)(2,1)}, bf16[128,8192]{1,0:T(8,128)(2,1)}, bf16[128,1024]{1,0:T(8,128)(2,1)}, f32[1024,1024]{1,0:T(8,128)}, f32[1024,1024]{1,0:T(8,128)}) custom-call(bf16[128,1024]{1,0:T(8,128)(2,1)} %xn.1, bf16[128,1024]{1,0:T(8,128)(2,1)} %xp.1, bf16[128,8192]{1,0:T(8,128)(2,1)} %hp.1, bf16[128,1024]{1,0:T(8,128)(2,1)} %ct.1, ...), custom_call_target="tpu_custom_call" | custom-call | tf_op jit(solution)/shard_map/pallas_call | solution.py:270
  190.1 0.0 copy-start.2
  190.1 0.0 copy-start.1
  190.1 1.8 copy.18
  191.9 3.1 %copy.19 = bf16[128,8192]{1,0:T(8,128)(2,1)} copy(bf16[128,8192]{1,0:T(8,128)(2,1)} %get-tuple-element.11) | data formatting | bytes 4194304
  195.0 0.0 copy-done.2
  195.0 0.7 copy.20
  195.7 0.0 copy-done.1
  195.7 0.0 copy-start
  195.7 2.1 %copy.21 = f32[1024,1024]{1,0:T(8,128)} copy(f32[1024,1024]{1,0:T(8,128)S(1)} %copy-done.1) | data formatting | bytes 8388608
  197.9 1.6 copy-done
  199.4 2.0 copy.22
Async XLA Ops:
  190.1 4.9 %copy-start.2 = (bf16[128,1024]{1,0:T(8,128)(2,1)S(1)}, bf16[128,1024]{1,0:T(8,128)(2,1)}, u32[]{:S(2)}) copy-start(bf16[128,1024]{1,0:T(8,128)(2,1)} %get-tuple-element.12) | copy-start | bytes 786436
  190.1 5.6 %copy-start.1 = (f32[1024,1024]{1,0:T(8,128)S(1)}, f32[1024,1024]{1,0:T(8,128)}, u32[]{:S(2)}) copy-start(f32[1024,1024]{1,0:T(8,128)} %get-tuple-element.13) | copy-start | bytes 12582916
  195.7 3.7 %copy-start = (f32[1024,1024]{1,0:T(8,128)S(1)}, f32[1024,1024]{1,0:T(8,128)}, u32[]{:S(2)}) copy-start(f32[1024,1024]{1,0:T(8,128)} %get-tuple-element.14) | copy-start | bytes 12582916

commit v2 on v1

--- a/solution.py
+++ b/solution.py
@@ -33,15 +33,17 @@
     xn, xp, hp, ct, uw, dw, ua_hbm, da_hbm,
     out, hn, ig, uo_hbm, do_hbm,
     x_all, c_all, p_all, hp_all, h_all, hg_all,
-    ht, bt, tp_h, tp_b, ot, it, ry_o, ry_i, ps_o, ps_i, rz_o, rz_i, ua, da,
+    ht, bt, tp_h, tp_b, ot, it, ry_o, ry_i, ps_o, ps_i, rr_o, rr_i, rz_o, rz_i, ua, da,
     x_s, x_r, c_s, c_r, p_s, p_r, hps_s, hps_r, hpt_s, hpt_r,
     th_s, th_r, tb_s, tb_r, ah_s, ah_r, ab_s, ab_r, hna_s, hna_r, hnt_s, hnt_r,
-    yo_s, yo_r, zo_s, zo_r, yi_s, yi_r, zi_s, zi_r, load_s, up_s, down_s,
+    yo_s, yo_r, zo_s, zo_r, yi_s, yi_r, zi_s, zi_r, ro_s, ro_r, ri_s, ri_r, load_s, up_s, down_s,
 ):
     f, t = lax.axis_index("fs"), lax.axis_index("tp")
     n_z = n_fs // PAIR
     z, y = f // PAIR, lax.rem(f, PAIR)
     mate = z * PAIR + (1 - y)
+    hs = n_z // 2
+    low, at_half = z // hs * hs, lax.rem(z, hs)
     rows, width = xn.shape[0], dw.shape[0]
     part = rows // n_tp
     mine = pl.ds(pl.multiple_of(t * part, part), part)
@@ -49,6 +51,14 @@
     def z_peer(k):
         return lax.rem(z + k, n_z)
 
+    def cross_of(zz):
+        return lax.rem(zz + hs, n_z)
+
+    cross = cross_of(z)
+
+    def half_peer(k):
+        return low + lax.rem(at_half + k, hs)
+
     def fs_peer(k):
         return lax.rem(f + k, n_fs)
 
@@ -70,22 +80,43 @@
     def landed(dst, send_sem, recv_sem, **target):
         send(dst, dst, send_sem, recv_sem, **target).wait_recv()
 
-    def gather_start(own, whole, ss, rs):
-        for k in range(1, n_z):
-            go(send(own, whole.at[f], ss.at[k], rs.at[f], fs=z_peer(k) * PAIR + y))
-        go(send(own, whole.at[f], ss.at[0], rs.at[f], fs=mate))
-
-    def gather_forward(own, whole, ss, rs):
-        whole[f] = own[...]
-        for k in range(1, n_z):
-            src = z_peer(k) * PAIR + y
-            landed(whole.at[src], ss.at[0], rs.at[src], fs=mate)
-            go(send(whole.at[src], whole.at[src], ss.at[n_z + k - 1], rs.at[src], fs=mate))
-
-    def gather_finish(whole, ss, rs):
-        for k in range(n_z):
-            src = z_peer(k) * PAIR + (1 - y)
-            landed(whole.at[src], ss.at[0], rs.at[src], fs=mate)
+    class Gather:
+        def __init__(self, own, whole, ss, rs):
+            self.own, self.whole, self.ss, self.rs, self.used = own, whole, ss, rs, 0
+
+        def put(self, src, block, g):
+            go(send(src, self.whole.at[block], self.ss.at[self.used], self.rs.at[block], fs=g))
+            self.used += 1
+
+        def wait(self, block):
+            landed(self.whole.at[block], self.ss.at[0], self.rs.at[block], fs=mate)
+
+        def start(self):
+            self.put(self.own, f, cross * PAIR + y)
+            for k in range(1, hs):
+                self.put(self.own, f, half_peer(k) * PAIR + y)
+            self.whole[f] = self.own[...]
+
+        def start_mate(self):
+            self.put(self.own, f, mate)
+
+        def relay(self):
+            block = cross * PAIR + y
+            self.wait(block)
+            for k in range(1, hs):
+                self.put(self.whole.at[block], block, half_peer(k) * PAIR + y)
+            self.put(self.whole.at[block], block, mate)
+
+        def forward(self):
+            for move in (lambda p: p, cross_of):
+                for k in range(1, hs):
+                    block = move(half_peer(k)) * PAIR + y
+                    self.wait(block)
+                    self.put(self.whole.at[block], block, mate)
+
+        def finish(self):
+            for k in range(n_z):
+                self.wait(z_peer(k) * PAIR + (1 - y))
 
     def tp_scatter(terms, held, ss, rs):
         for k in range(1, n_tp):
@@ -120,26 +151,57 @@
             total = contract(left, right[...], 1, right_dim).astype(BF16)
             terms[pl.ds(i * PAIR, PAIR)] = total.reshape(PAIR, rows, total.shape[-1])
 
-    def scatter_start(terms, ry, ss, rs):
-        for k in range(n_z):
-            zz = z_peer((k + 1) % n_z)
-            go(send(terms.at[zz * PAIR + (1 - y)], ry.at[zz], ss.at[k], rs.at[zz], fs=mate))
-
-    def scatter_pass(terms, ry, ps, rz, ss, rs, zs, zr):
-        for k in range(1, n_z):
-            zz = z_peer(k)
-            landed(ry.at[zz], ss.at[0], rs.at[zz], fs=mate)
-            ps[zz] = (terms[zz * PAIR + y].astype(F32) + ry[zz].astype(F32)).astype(BF16)
-            go(send(ps.at[zz], rz.at[z], zs.at[k], zr.at[z], fs=zz * PAIR + y))
-
-    def scatter_finish(terms, ry, rz, ss, rs, zs, zr, result):
-        landed(ry.at[z], ss.at[0], rs.at[z], fs=mate)
-        total = terms[f].astype(F32) + ry[z].astype(F32)
-        for k in range(1, n_z):
-            zz = z_peer(k)
-            landed(rz.at[zz], zs.at[0], zr.at[zz], fs=zz * PAIR + y)
-            total = total + rz[zz].astype(F32)
-        result[...] = total.astype(BF16)
+    class Scatter:
+        def __init__(self, terms, ry, ps, rr, rz, sems):
+            self.terms, self.ry, self.ps, self.rr, self.rz = terms, ry, ps, rr, rz
+            self.ys, self.yr, self.rs, self.rrecv, self.zs, self.zr = sems
+
+        def start(self):
+            order = [cross_of(half_peer(k)) for k in range(1, hs)] + [cross]
+            order += [half_peer(k) for k in range(1, hs)] + [z]
+            for k, zz in enumerate(order):
+                block = self.terms.at[zz * PAIR + (1 - y)]
+                go(send(block, self.ry.at[zz], self.ys.at[k], self.yr.at[zz], fs=mate))
+
+        def pair(self, zz):
+            landed(self.ry.at[zz], self.ys.at[0], self.yr.at[zz], fs=mate)
+            return self.terms[zz * PAIR + y].astype(F32) + self.ry[zz].astype(F32)
+
+        def spread(self):
+            for k in range(1, hs):
+                p = half_peer(k)
+                zz = cross_of(p)
+                self.ps[zz] = self.pair(zz).astype(BF16)
+                slot, sem = self.rr.at[at_half], self.rrecv.at[at_half]
+                go(send(self.ps.at[zz], slot, self.rs.at[k], sem, fs=p * PAIR + y))
+
+        def relay(self):
+            total = self.pair(cross)
+            for k in range(1, hs):
+                p = half_peer(k)
+                w = p - low
+                landed(self.rr.at[w], self.rs.at[0], self.rrecv.at[w], fs=p * PAIR + y)
+                total = total + self.rr[w].astype(F32)
+            self.ps[cross] = total.astype(BF16)
+            go(send(
+                self.ps.at[cross], self.rz.at[hs], self.zs.at[0], self.zr.at[hs],
+                fs=cross * PAIR + y,
+            ))
+            for k in range(1, hs):
+                p = half_peer(k)
+                self.ps[p] = self.pair(p).astype(BF16)
+                slot, sem = self.rz.at[at_half], self.zr.at[at_half]
+                go(send(self.ps.at[p], slot, self.zs.at[k], sem, fs=p * PAIR + y))
+
+        def finish(self, result):
+            total = self.pair(z)
+            for k in range(1, hs):
+                p = half_peer(k)
+                w = p - low
+                landed(self.rz.at[w], self.zs.at[0], self.zr.at[w], fs=p * PAIR + y)
+                total = total + self.rz[w].astype(F32)
+            landed(self.rz.at[hs], self.zs.at[0], self.zr.at[hs], fs=cross * PAIR + y)
+            result[...] = (total + self.rz[hs].astype(F32)).astype(BF16)
 
     barrier = pltpu.get_barrier_semaphore()
     for k in range(1, n_fs):
@@ -152,11 +214,14 @@
         )
     pl.semaphore_wait(barrier, n_fs + n_tp - 2)
 
-    gather_start(xn, x_all, x_s, x_r)
-    gather_start(ct, c_all, c_s, c_r)
-    for k in range(1, n_fs):
-        g = fs_peer(k)
-        go(send(hp.at[mine, unit(g)], hp_all.at[f, mine, :], hps_s.at[k], hps_r.at[f], fs=g))
+    gx = Gather(xn, x_all, x_s, x_r)
+    gc = Gather(ct, c_all, c_s, c_r)
+    gp = Gather(xp, p_all, p_s, p_r)
+    sum_o = Scatter(ot, ry_o, ps_o, rr_o, rz_o, (yo_s, yo_r, ro_s, ro_r, zo_s, zo_r))
+    sum_i = Scatter(it, ry_i, ps_i, rr_i, rz_i, (yi_s, yi_r, ri_s, ri_r, zi_s, zi_r))
+
+    gx.start()
+    gx.start_mate()
     loads = [
         pltpu.make_async_copy(ua_hbm, ua, load_s.at[0]),
         pltpu.make_async_copy(da_hbm, da, load_s.at[1]),
@@ -164,11 +229,19 @@
     for load in loads:
         load.start()
     hp_all[f, mine, :] = hp[mine, unit(f)]
-
-    gather_forward(xn, x_all, x_s, x_r)
-    gather_finish(x_all, x_s, x_r)
+    gx.relay()
+    gc.start()
+    gx.forward()
+    gc.start_mate()
+    gc.relay()
+    for k in range(1, n_fs):
+        g = fs_peer(k)
+        go(send(hp.at[mine, unit(g)], hp_all.at[f, mine, :], hps_s.at[k], hps_r.at[f], fs=g))
+
+    gx.finish()
     products(lambda at: x_all[at], uw, 0, ht)
     tp_scatter(ht, tp_h, th_s, th_r)
+    gc.forward()
     tp_scatter_wait(tp_h, th_s, th_r)
 
     @pl.loop(0, n_fs)
@@ -182,12 +255,10 @@
     hn[mine, unit(f)] = h_all[f, mine, :]
     tp_gather_wait(lambda at: h_all.at[:, at, :], ah_s, ah_r)
     products(lambda at: relu_squared(h_all[at]), dw, 0, ot)
-    scatter_start(ot, ry_o, yo_s, yo_r)
-
-    gather_forward(ct, c_all, c_s, c_r)
-    gather_start(xp, p_all, p_s, p_r)
-    scatter_pass(ot, ry_o, ps_o, rz_o, yo_s, yo_r, zo_s, zo_r)
-    gather_finish(c_all, c_s, c_r)
+    sum_o.start()
+    gp.start()
+
+    gc.finish()
     products(lambda at: c_all[at], dw, 1, bt)
     tp_scatter(bt, tp_b, tb_s, tb_r)
     for k in range(1, n_fs):
@@ -204,8 +275,12 @@
     tp_gather(lambda at: hg_all.at[:, at, :], ab_s, ab_r)
     tp_gather_wait(lambda at: hg_all.at[:, at, :], ab_s, ab_r)
     products(lambda at: hg_all[at], uw, 1, it)
-    scatter_start(it, ry_i, yi_s, yi_r)
-    gather_forward(xp, p_all, p_s, p_r)
+    sum_i.start()
+    sum_o.spread()
+    sum_o.relay()
+    gp.start_mate()
+    gp.relay()
+    gp.forward()
 
     tp_gather_wait(lambda at: hp_all.at[:, at, :], hpt_s, hpt_r)
     for load in loads:
@@ -234,16 +309,17 @@
     drain_down = accumulate(
         lambda at: relu_squared(hp_all[:, :, at]), c_all, da, do_hbm, down_s, n_down
     )
-    scatter_pass(it, ry_i, ps_i, rz_i, yi_s, yi_r, zi_s, zi_r)
+    sum_i.spread()
+    sum_i.relay()
 
     for k in range(1, n_fs):
         g = fs_peer(k)
         landed(hn.at[mine, unit(g)], hna_s.at[0], hna_r.at[g], fs=g)
     tp_gather(lambda at: hn.at[at, :], hnt_s, hnt_r)
-    scatter_finish(ot, ry_o, rz_o, yo_s, yo_r, zo_s, zo_r, out)
-    gather_finish(p_all, p_s, p_r)
+    sum_o.finish(out)
+    gp.finish()
     drain_up = accumulate(lambda at: p_all[:, :, at], hg_all, ua, uo_hbm, up_s, n_up)
-    scatter_finish(it, ry_i, rz_i, yi_s, yi_r, zi_s, zi_r, ig)
+    sum_i.finish(ig)
     tp_gather_wait(lambda at: hn.at[at, :], hnt_s, hnt_r)
     drain_down()
     drain_up()
@@ -286,12 +362,14 @@
             tokens(depth), tokens(depth),
             held(n_z, rows, depth), held(n_z, rows, depth),
             held(n_z, rows, depth), held(n_z, rows, depth),
-            held(n_z, rows, depth), held(n_z, rows, depth),
+            held(n_z // 2, rows, depth), held(n_z // 2, rows, depth),
+            held(n_z // 2 + 1, rows, depth), held(n_z // 2 + 1, rows, depth),
             held(*ua.shape, dtype=F32), held(*da.shape, dtype=F32),
             fs_sem, fs_sem, fs_sem, fs_sem, fs_sem, fs_sem, fs_sem, fs_sem, tp_sem, tp_sem,
             tp_sem, tp_sem, tp_sem, tp_sem, tp_sem, tp_sem, tp_sem, tp_sem,
             fs_sem, fs_sem, tp_sem, tp_sem,
             z_sem, z_sem, z_sem, z_sem, z_sem, z_sem, z_sem, z_sem,
+            z_sem, z_sem, z_sem, z_sem,
             dma((2,)), dma((n_up,)), dma((n_down,)),
         ],
         compiler_params=pltpu.CompilerParams(

time: 202 us -> 171 us (0.85)
  the two profiles are of different devices: /device:TPU:14 before, /device:TPU:0 now
where the time goes in v2:
time: 171 us
  Pallas kernels  159 us (93%)
  local copies, waits for them, and re-layouts  11.3 us (7%)
    pallas_call x1, Pallas kernels, local(): pl.pallas_call(functools.partial(kernel, n_fs, n_tp, n_up, n_down), out_s...  159 us
    unnamed x11, local copies, waits for them, and re-layouts  11.3 us

profile of v2, /device:TPU:0, one launch (start us, length us, event | category | flops | bytes accessed | tf_op | source)
XLA Modules:
  0.0 171.1 jit_solution(2460608556678088913)
XLA Ops:
  0.6 159.1 %shard_map.119 = (bf16[128,1024]{1,0:T(8,128)(2,1)}, bf16[128,8192]{1,0:T(8,128)(2,1)}, bf16[128,1024]{1,0:T(8,128)(2,1)}, f32[1024,1024]{1,0:T(8,128)}, f32[1024,1024]{1,0:T(8,128)}) custom-call(bf16[128,1024]{1,0:T(8,128)(2,1)} %xn.1, bf16[128,1024]{1,0:T(8,128)(2,1)} %xp.1, bf16[128,8192]{1,0:T(8,128)(2,1)} %hp.1, bf16[128,1024]{1,0:T(8,128)(2,1)} %ct.1, ...), custom_call_target="tpu_custom_call" | custom-call | tf_op jit(solution)/shard_map/pallas_call | solution.py:346
  159.8 0.0 copy-start.2
  159.8 0.0 copy-start.1
  159.8 1.8 %copy.18 = bf16[128,1024]{1,0:T(8,128)(2,1)} copy(bf16[128,1024]{1,0:T(8,128)(2,1)} %get-tuple-element.10) | data formatting | bytes 524288
  161.6 3.1 %copy.19 = bf16[128,8192]{1,0:T(8,128)(2,1)} copy(bf16[128,8192]{1,0:T(8,128)(2,1)} %get-tuple-element.11) | data formatting | bytes 4194304
  164.7 0.0 copy-done.2
  164.7 0.7 copy.20
  165.4 0.0 copy-done.1
  165.4 0.0 copy-start
  165.4 2.1 %copy.21 = f32[1024,1024]{1,0:T(8,128)} copy(f32[1024,1024]{1,0:T(8,128)S(1)} %copy-done.1) | data formatting | bytes 8388608
  167.6 1.6 copy-done
  169.1 2.0 %copy.22 = f32[1024,1024]{1,0:T(8,128)} copy(f32[1024,1024]{1,0:T(8,128)S(1)} %copy-done) | data formatting | bytes 8388608
Async XLA Ops:
  159.8 4.9 %copy-start.2 = (bf16[128,1024]{1,0:T(8,128)(2,1)S(1)}, bf16[128,1024]{1,0:T(8,128)(2,1)}, u32[]{:S(2)}) copy-start(bf16[128,1024]{1,0:T(8,128)(2,1)} %get-tuple-element.12) | copy-start | bytes 786436
  159.8 5.6 %copy-start.1 = (f32[1024,1024]{1,0:T(8,128)S(1)}, f32[1024,1024]{1,0:T(8,128)}, u32[]{:S(2)}) copy-start(f32[1024,1024]{1,0:T(8,128)} %get-tuple-element.13) | copy-start | bytes 12582916
  165.4 3.7 %copy-start = (f32[1024,1024]{1,0:T(8,128)S(1)}, f32[1024,1024]{1,0:T(8,128)}, u32[]{:S(2)}) copy-start(f32[1024,1024]{1,0:T(8,128)} %get-tuple-element.14) | copy-start | bytes 12582916

commit v3 on v2

--- a/solution.py
+++ b/solution.py
@@ -29,14 +29,15 @@
 
 
 def kernel(
-    n_fs, n_tp, n_up, n_down,
-    xn, xp, hp, ct, uw, dw, ua_hbm, da_hbm,
-    out, hn, ig, uo_hbm, do_hbm,
+    n_fs, n_tp,
+    xn_hbm, xp_hbm, hp_hbm, ct_hbm, uw_hbm, dw_hbm, ua_hbm, da_hbm,
+    out, hn, ig, ua, da,
+    xn, xp, hp, ct, uw, dw,
     x_all, c_all, p_all, hp_all, h_all, hg_all,
-    ht, bt, tp_h, tp_b, ot, it, ry_o, ry_i, ps_o, ps_i, rr_o, rr_i, rz_o, rz_i, ua, da,
+    ht, bt, tp_h, tp_b, ot, it, ry_o, ry_i, ps_o, ps_i, rr_o, rr_i, rz_o, rz_i,
     x_s, x_r, c_s, c_r, p_s, p_r, hps_s, hps_r, hpt_s, hpt_r,
     th_s, th_r, tb_s, tb_r, ah_s, ah_r, ab_s, ab_r, hna_s, hna_r, hnt_s, hnt_r,
-    yo_s, yo_r, zo_s, zo_r, yi_s, yi_r, zi_s, zi_r, ro_s, ro_r, ri_s, ri_r, load_s, up_s, down_s,
+    yo_s, yo_r, zo_s, zo_r, yi_s, yi_r, zi_s, zi_r, ro_s, ro_r, ri_s, ri_r, load_s,
 ):
     f, t = lax.axis_index("fs"), lax.axis_index("tp")
     n_z = n_fs // PAIR
@@ -203,6 +204,15 @@
             landed(self.rz.at[hs], self.zs.at[0], self.zr.at[hs], fs=cross * PAIR + y)
             result[...] = (total + self.rz[hs].astype(F32)).astype(BF16)
 
+    def load(k, src, dst):
+        copy = pltpu.make_async_copy(src, dst, load_s.at[k])
+        copy.start()
+        return copy
+
+    load_xn, load_ct, load_xp = load(0, xn_hbm, xn), load(1, ct_hbm, ct), load(2, xp_hbm, xp)
+    load_hp, load_uw, load_dw = load(3, hp_hbm, hp), load(4, uw_hbm, uw), load(5, dw_hbm, dw)
+    load_ua, load_da = load(6, ua_hbm, ua), load(7, da_hbm, da)
+
     barrier = pltpu.get_barrier_semaphore()
     for k in range(1, n_fs):
         pl.semaphore_signal(
@@ -220,19 +230,19 @@
     sum_o = Scatter(ot, ry_o, ps_o, rr_o, rz_o, (yo_s, yo_r, ro_s, ro_r, zo_s, zo_r))
     sum_i = Scatter(it, ry_i, ps_i, rr_i, rz_i, (yi_s, yi_r, ri_s, ri_r, zi_s, zi_r))
 
+    load_xn.wait()
     gx.start()
     gx.start_mate()
-    loads = [
-        pltpu.make_async_copy(ua_hbm, ua, load_s.at[0]),
-        pltpu.make_async_copy(da_hbm, da, load_s.at[1]),
-    ]
-    for load in loads:
-        load.start()
+    load_ct.wait()
+    gc.start_mate()
+    load_xp.wait()
+    load_hp.wait()
     hp_all[f, mine, :] = hp[mine, unit(f)]
+    load_uw.wait()
+    load_dw.wait()
     gx.relay()
     gc.start()
     gx.forward()
-    gc.start_mate()
     gc.relay()
     for k in range(1, n_fs):
         g = fs_peer(k)
@@ -283,32 +293,30 @@
     gp.forward()
 
     tp_gather_wait(lambda at: hp_all.at[:, at, :], hpt_s, hpt_r)
-    for load in loads:
-        load.wait()
-
-    def accumulate(left_of, right, total, hbm, sems, pieces):
-        high = total.shape[0] // pieces
-
-        def piece(i):
-            return pl.ds(pl.multiple_of(i * high, high), high)
-
-        @pl.loop(0, pieces)
+    load_ua.wait()
+    load_da.wait()
+
+    def accumulate(left_of, right, total):
+        high = min(total.shape[0], 256)
+
+        @pl.loop(0, total.shape[0] // high)
         def _(i):
-            left = left_of(piece(i)).reshape(n_fs * rows, high)
-            flat = right[...].reshape(n_fs * rows, right.shape[-1])
-            total[piece(i), :] += contract(left, flat, 0, 0)
-            pltpu.make_async_copy(total.at[piece(i), :], hbm.at[piece(i), :], sems.at[i]).start()
-
-        def drain():
-            for i in range(pieces):
-                at = pl.ds(i * high, high)
-                pltpu.make_async_copy(total.at[at, :], hbm.at[at, :], sems.at[i]).wait()
-
-        return drain
-
-    drain_down = accumulate(
-        lambda at: relu_squared(hp_all[:, :, at]), c_all, da, do_hbm, down_s, n_down
-    )
+            at = pl.ds(pl.multiple_of(i * high, high), high)
+            total[at, :] += contract(left_of(at), right(), 0, 0)
+
+    def flat(values):
+        return values.reshape(n_fs * rows, values.shape[-1])
+
+    def accumulate_up(side):
+        blocks = [k * PAIR + side for k in range(n_z)]
+        accumulate(
+            lambda at: jnp.concatenate([p_all[b, :, at] for b in blocks]),
+            lambda: jnp.concatenate([hg_all[b] for b in blocks]),
+            ua,
+        )
+
+    accumulate(lambda at: flat(relu_squared(hp_all[:, :, at])), lambda: flat(c_all[...]), da)
+    accumulate_up(y)
     sum_i.spread()
     sum_i.relay()
 
@@ -318,11 +326,9 @@
     tp_gather(lambda at: hn.at[at, :], hnt_s, hnt_r)
     sum_o.finish(out)
     gp.finish()
-    drain_up = accumulate(lambda at: p_all[:, :, at], hg_all, ua, uo_hbm, up_s, n_up)
+    accumulate_up(1 - y)
     sum_i.finish(ig)
     tp_gather_wait(lambda at: hn.at[at, :], hnt_s, hnt_r)
-    drain_down()
-    drain_up()
     for copy in sent:
         copy.wait_send()
 
@@ -332,7 +338,6 @@
     width = dw.shape[0]
     n_z = n_fs // PAIR
     part = rows // n_tp
-    n_up, n_down = max(1, depth // 256), max(1, width // 256)
     dma = pltpu.SemaphoreType.DMA
 
     def held(*shape, dtype=BF16):
@@ -341,20 +346,22 @@
     def tokens(columns):
         return held(n_fs, rows, columns)
 
-    vmem, anywhere = pl.BlockSpec(memory_space=pltpu.VMEM), pl.BlockSpec(memory_space=pl.ANY)
+    vmem, hbm = pl.BlockSpec(memory_space=pltpu.VMEM), pl.BlockSpec(memory_space=pltpu.HBM)
     fs_sem, tp_sem, z_sem = dma((n_fs,)), dma((n_tp,)), dma((n_z,))
     return pl.pallas_call(
-        functools.partial(kernel, n_fs, n_tp, n_up, n_down),
+        functools.partial(kernel, n_fs, n_tp),
         out_shape=(
-            jax.ShapeDtypeStruct(xn.shape, BF16),
-            jax.ShapeDtypeStruct(hp.shape, BF16),
-            jax.ShapeDtypeStruct(xp.shape, BF16),
-            jax.ShapeDtypeStruct(ua.shape, F32),
-            jax.ShapeDtypeStruct(da.shape, F32),
+            pltpu.VMEM(xn.shape, BF16),
+            pltpu.VMEM(hp.shape, BF16),
+            pltpu.VMEM(xp.shape, BF16),
+            pltpu.VMEM(ua.shape, F32),
+            pltpu.VMEM(da.shape, F32),
         ),
-        in_specs=[vmem] * 6 + [anywhere] * 2,
-        out_specs=(vmem, vmem, vmem, anywhere, anywhere),
+        in_specs=[hbm] * 8,
+        out_specs=(vmem,) * 5,
         scratch_shapes=[
+            held(rows, depth), held(rows, depth), held(*hp.shape), held(rows, depth),
+            held(*uw.shape), held(*dw.shape),
             tokens(depth), tokens(depth), tokens(depth),
             tokens(width), tokens(width), tokens(width),
             tokens(width), tokens(width),
@@ -364,16 +371,15 @@
             held(n_z, rows, depth), held(n_z, rows, depth),
             held(n_z // 2, rows, depth), held(n_z // 2, rows, depth),
             held(n_z // 2 + 1, rows, depth), held(n_z // 2 + 1, rows, depth),
-            held(*ua.shape, dtype=F32), held(*da.shape, dtype=F32),
             fs_sem, fs_sem, fs_sem, fs_sem, fs_sem, fs_sem, fs_sem, fs_sem, tp_sem, tp_sem,
             tp_sem, tp_sem, tp_sem, tp_sem, tp_sem, tp_sem, tp_sem, tp_sem,
             fs_sem, fs_sem, tp_sem, tp_sem,
             z_sem, z_sem, z_sem, z_sem, z_sem, z_sem, z_sem, z_sem,
             z_sem, z_sem, z_sem, z_sem,
-            dma((2,)), dma((n_up,)), dma((n_down,)),
+            dma((8,)),
         ],
         compiler_params=pltpu.CompilerParams(
-            collective_id=0, has_side_effects=True, vmem_limit_bytes=62 * 1024 * 1024
+            collective_id=0, has_side_effects=True, vmem_limit_bytes=52 * 1024 * 1024
         ),
     )(xn, xp, hp, ct, uw, dw, ua, da)
 

time: 171 us -> 154 us (0.901)
  Pallas kernels: 159 us -> 147 us
  local copies, waits for them, and re-layouts: 11.3 us -> 6.75 us
    pallas_call x1, Pallas kernels: 159 us -> 147 us  [local(): pl.pallas_call(functools.partial(kernel, n_fs, n_tp), out_shape=(pltpu.VM...]
    unnamed x11 -> x5, local copies, waits for them, and re-layouts: 11.3 us -> 6.75 us
where the time goes in v3:
time: 154 us
  Pallas kernels  147 us (95%)
  local copies, waits for them, and re-layouts  6.75 us (4%)
    pallas_call x1, Pallas kernels, local(): pl.pallas_call(functools.partial(kernel, n_fs, n_tp), out_shape=(pltpu.VM...  147 us
    unnamed x5, local copies, waits for them, and re-layouts  6.75 us

profile of v3, /device:TPU:0, one launch (start us, length us, event | category | flops | bytes accessed | tf_op | source)
XLA Modules:
  0.0 154.3 jit_solution(4099892930533778619)
XLA Ops:
  0.6 146.9 %shard_map.119 = (bf16[128,1024]{1,0:T(8,128)(2,1)S(1)}, bf16[128,8192]{1,0:T(8,128)(2,1)S(1)}, bf16[128,1024]{1,0:T(8,128)(2,1)S(1)}, f32[1024,1024]{1,0:T(8,128)S(1)}, f32[1024,1024]{1,0:T(8,128)S(1)}) custom-call(bf16[128,1024]{1,0:T(8,128)(2,1)} %xn_hbm.1, bf16[128,1024]{1,0:T(8,128)(2,1)} %xp_hbm.1, bf16[128,8192]{1,0:T(8,128)(2,1)} %hp_hbm.1, ...), custom_call_target="tpu_custom_call" | custom-call | tf_op jit(solution)/shard_map/pallas_call | solution.py:351
  147.6 0.7 copy.18
  148.3 0.7 copy.20
  149.0 1.3 copy.19
  150.3 2.0 %copy.21 = f32[1024,1024]{1,0:T(8,128)} copy(f32[1024,1024]{1,0:T(8,128)S(1)} %get-tuple-element.8) | data formatting | bytes 8388608
  152.3 2.0 %copy.22 = f32[1024,1024]{1,0:T(8,128)} copy(f32[1024,1024]{1,0:T(8,128)S(1)} %get-tuple-element.9) | data formatting | bytes 8388608

commit v4 on v3

--- a/solution.py
+++ b/solution.py
@@ -115,8 +115,19 @@
                     self.wait(block)
                     self.put(self.whole.at[block], block, mate)
 
-        def finish(self):
-            for k in range(n_z):
+        def forward_wide(self):
+            self.wait(mate)
+            for k in range(1, hs):
+                self.put(self.whole.at[mate], mate, half_peer(k) * PAIR + y)
+            for k in range(1, hs):
+                self.wait(half_peer(k) * PAIR + y)
+            for k in range(1, hs):
+                block = cross_of(half_peer(k)) * PAIR + y
+                self.wait(block)
+                self.put(self.whole.at[block], block, mate)
+
+        def finish(self, first=0):
+            for k in range(first, n_z):
                 self.wait(z_peer(k) * PAIR + (1 - y))
 
     def tp_scatter(terms, held, ss, rs):
@@ -241,6 +252,7 @@
     load_uw.wait()
     load_dw.wait()
     gx.relay()
+    gp.start_mate()
     gc.start()
     gx.forward()
     gc.relay()
@@ -288,9 +300,8 @@
     sum_i.start()
     sum_o.spread()
     sum_o.relay()
-    gp.start_mate()
     gp.relay()
-    gp.forward()
+    gp.forward_wide()
 
     tp_gather_wait(lambda at: hp_all.at[:, at, :], hpt_s, hpt_r)
     load_ua.wait()
@@ -325,12 +336,21 @@
         landed(hn.at[mine, unit(g)], hna_s.at[0], hna_r.at[g], fs=g)
     tp_gather(lambda at: hn.at[at, :], hnt_s, hnt_r)
     sum_o.finish(out)
-    gp.finish()
+    gp.finish(1)
     accumulate_up(1 - y)
     sum_i.finish(ig)
     tp_gather_wait(lambda at: hn.at[at, :], hnt_s, hnt_r)
     for copy in sent:
         copy.wait_send()
+
+
+def write_out(*refs):
+    sems = refs[-1]
+    copies = [pltpu.make_async_copy(refs[k], refs[5 + k], sems.at[k]) for k in (3, 4, 1, 0, 2)]
+    for copy in copies:
+        copy.start()
+    for copy in copies:
+        copy.wait()
 
 
 def local(n_fs, n_tp, xn, xp, hp, ct, uw, dw, ua, da):
@@ -348,7 +368,7 @@
 
     vmem, hbm = pl.BlockSpec(memory_space=pltpu.VMEM), pl.BlockSpec(memory_space=pltpu.HBM)
     fs_sem, tp_sem, z_sem = dma((n_fs,)), dma((n_tp,)), dma((n_z,))
-    return pl.pallas_call(
+    results = pl.pallas_call(
         functools.partial(kernel, n_fs, n_tp),
         out_shape=(
             pltpu.VMEM(xn.shape, BF16),
@@ -382,6 +402,14 @@
             collective_id=0, has_side_effects=True, vmem_limit_bytes=52 * 1024 * 1024
         ),
     )(xn, xp, hp, ct, uw, dw, ua, da)
+    return pl.pallas_call(
+        write_out,
+        out_shape=tuple(jax.ShapeDtypeStruct(r.shape, r.dtype) for r in results),
+        in_specs=[pl.BlockSpec(memory_space=pl.ANY)] * 5,
+        out_specs=(hbm,) * 5,
+        scratch_shapes=[dma((5,))],
+        compiler_params=pltpu.CompilerParams(vmem_limit_bytes=1024 * 1024),
+    )(*results)
 
 
 def solution(mesh):

time: 154 us -> 149 us (0.968)
  local copies, waits for them, and re-layouts: 6.75 us -> 0 us
    unnamed x5 -> x0, local copies, waits for them, and re-layouts: 6.75 us -> none
    pallas_call x0 -> x1, Pallas kernels: none -> 4.1 us  [local(): pl.pallas_call(write_out, out_shape=tuple((jax.ShapeDtypeStruct(r.shape,...]
    pallas_call x1, Pallas kernels: 147 us -> 144 us  [local(): pl.pallas_call(functools.partial(kernel, n_fs, n_tp), out_shape=(pltpu.VM...]
where the time goes in v4:
time: 149 us
  Pallas kernels  148 us (99%)
    pallas_call x1, Pallas kernels, local(): pl.pallas_call(functools.partial(kernel, n_fs, n_tp), out_shape=(pltpu.VM...  144 us
    pallas_call x1, Pallas kernels, local(): pl.pallas_call(write_out, out_shape=tuple((jax.ShapeDtypeStruct(r.shape,...  4.1 us

profile of v4, /device:TPU:0, one launch (start us, length us, event | category | flops | bytes accessed | tf_op | source)
XLA Modules:
  0.0 149.1 jit_solution(15126177140923562349)
XLA Ops:
  0.6 144.4 %shard_map.119 = (bf16[128,1024]{1,0:T(8,128)(2,1)S(1)}, bf16[128,8192]{1,0:T(8,128)(2,1)S(1)}, bf16[128,1024]{1,0:T(8,128)(2,1)S(1)}, f32[1024,1024]{1,0:T(8,128)S(1)}, f32[1024,1024]{1,0:T(8,128)S(1)}) custom-call(bf16[128,1024]{1,0:T(8,128)(2,1)} %xn_hbm.1, bf16[128,1024]{1,0:T(8,128)(2,1)} %xp_hbm.1, bf16[128,8192]{1,0:T(8,128)(2,1)} %hp_hbm.1, ...), custom_call_target="tpu_custom_call" | custom-call | tf_op jit(solution)/shard_map/pallas_call | solution.py:371
  145.0 4.1 %shard_map.120 = (bf16[128,1024]{1,0:T(8,128)(2,1)}, bf16[128,8192]{1,0:T(8,128)(2,1)}, bf16[128,1024]{1,0:T(8,128)(2,1)}, f32[1024,1024]{1,0:T(8,128)}, f32[1024,1024]{1,0:T(8,128)}) custom-call(bf16[128,1024]{1,0:T(8,128)(2,1)S(1)} %get-tuple-element.10.refs_0_, bf16[128,8192]{1,0:T(8,128)(2,1)S(1)} %get-tuple-element.11.refs_1_, ...), custom_call_target="tpu_custom_call" | custom-call | tf_op jit(solution)/shard_map/pallas_call | solution.py:405
